TPU v7x, 32 devices: a whole 2x2x4 slice. The times are simulated.
32 devices in a mesh: grp: 2 (over x), ep: 4 (over y, core), tp: 4 (over z).
Axes of the slice: x: 2, y: 2, z: 4, core: 2. Of those that a mesh axis runs over, the one named last changes fastest.
Arguments:
- pool_input: bfloat16 [8192, 1024], P(('grp', 'ep'), 'tp'), parts along dimension 0, may hold values from -6 to 6
- pool_map: bfloat16 [8, 128, 128], replicated, may hold values from -0.5 to 0.5
- pool_scale: float32 [1024], replicated, may hold values from 0.1 to 1.9
- out_weight: bfloat16 [1024, 2048], P(None, 'tp'), may hold values from -0.1875 to 0.1875
- expert_input: bfloat16 [4096, 2048], P(('grp', 'ep', 'tp')), parts along dimension 0, may hold values from -6 to 6
- norm_gain: float32 [2048], replicated, may hold values from 0.1 to 1.9
- routes: int32 [4096, 2], P(('grp', 'ep', 'tp')), parts along dimension 0, may hold values from 0 to 15, all different within a row; in each aligned block of 128 rows (0 to 127, 128 to 255, ...) at most 32 rows name the same one
- route_weight: float32 [4096, 2], P(('grp', 'ep', 'tp')), parts along dimension 0, may hold values from 0.2 to 1.5
- gate_weight: bfloat16 [16, 2048, 512], P(('ep', 'tp')), may hold values from -0.125 to 0.125
- up_weight: bfloat16 [16, 2048, 512], P(('ep', 'tp')), may hold values from -0.125 to 0.125
- down_weight: bfloat16 [16, 512, 2048], P(('ep', 'tp')), may hold values from -0.25 to 0.25
Outputs:
- pool_output: bfloat16 [8192, 2048], P(('grp', 'ep'), 'tp'), parts along dimension 0
- expert_output: bfloat16 [4096, 2048], P(('grp', 'ep', 'tp')), parts along dimension 0
There are 2 independent parts, one for each index of `grp`. A program takes and returns all parts, laid end to end along the dimension named above; an argument that names none is the same for every part. Nothing has to cross between parts.
Inputs may be any that keep to these rules, and one draw needn't show every extreme that they name: `routes`: each row names 2 different experts. In the rows of one device no expert is named more than 32 times, and in every draw some device names some expert exactly 32 times.
All inputs are finite; a program needn't handle non-finite values.
Results may differ from a plain program's by a relative error of at most 0.007.
Values may be sent and summed in bfloat16 or wider, within the bound.
No kernel may reach another device: no remote copies, remote signals or barrier semaphores. Data moves between devices by JAX's collectives and lax.ppermute only.
A program may use at most 64 MiB of HBM per device.

v0:
```python
import jax
import jax.numpy as jnp
from jax import lax
from jax.sharding import PartitionSpec as P

epsilon = 1e-06
halo_depth = 16


def shifted_2(shard, axis, by):
    size = lax.axis_size(axis)
    pairs = [(i, i + by) for i in range(size) if 0 <= i + by < size]
    return lax.ppermute(shard, axis, pairs)


def expert_rows(received, gate_weight, up_weight, down_weight):
    shape_in = received.shape
    flat_rows = received.reshape(-1, shape_in[-1])
    gate_part = jnp.dot(flat_rows, gate_weight[0], preferred_element_type=jnp.float32)
    up_part = jnp.dot(flat_rows, up_weight[0], preferred_element_type=jnp.float32)
    hidden = (jax.nn.silu(gate_part) * up_part).astype(jnp.bfloat16)
    result = jnp.dot(hidden, down_weight[0], preferred_element_type=jnp.float32).astype(
        jnp.bfloat16
    )
    return result.reshape(shape_in)


def pool_half(pool_input, pool_map, pool_scale, out_weight):
    row_count, width_local = pool_input.shape
    group_dim = pool_map.shape[1]
    groups_local = width_local // group_dim
    last_rows = pool_input[row_count - halo_depth :]
    earlier_rows = shifted_2(last_rows, "ep", 1)
    extended = jnp.concatenate([earlier_rows, pool_input], axis=0).astype(jnp.float32)
    first_group = lax.axis_index("tp") * groups_local
    group_ids = first_group + jnp.arange(width_local, dtype=jnp.int32) // group_dim
    window = jnp.left_shift(jnp.int32(2), group_ids % 4)
    summed = jnp.zeros((row_count, width_local), jnp.float32)
    for offset in range(halo_depth):
        shifted = extended[halo_depth - offset : halo_depth - offset + row_count]
        summed = summed + jnp.where(offset < window, shifted, 0.0)
    positions = lax.axis_index("ep") * row_count + jnp.arange(row_count, dtype=jnp.int32)
    counted = jnp.minimum(positions[:, None] + 1, window[None, :]).astype(jnp.float32)
    pooled = (summed / counted - extended[halo_depth:]).astype(jnp.bfloat16)
    maps_local = lax.dynamic_slice_in_dim(pool_map, first_group, groups_local, 0)
    scales_local = lax.dynamic_slice_in_dim(pool_scale, first_group * group_dim, width_local, 0)
    mapped = jnp.einsum(
        "rgc,gcd->rgd",
        pooled.reshape(row_count, groups_local, group_dim),
        maps_local,
        preferred_element_type=jnp.float32,
    )
    mapped = (mapped.reshape(row_count, width_local) * scales_local).astype(jnp.bfloat16)
    projected = jnp.dot(
        lax.all_gather(mapped, "tp", axis=1, tiled=True),
        out_weight,
        preferred_element_type=jnp.float32,
    )
    return projected.astype(jnp.bfloat16)


def expert_half(expert_input, norm_gain, routes, route_weight, gate_weight, up_weight, down_weight):
    row_count, model_width = expert_input.shape
    top_count = routes.shape[1]
    widened = expert_input.astype(jnp.float32)
    normed = (
        widened
        * lax.rsqrt(jnp.mean(widened * widened, axis=1, keepdims=True) + epsilon)
        * norm_gain
    )
    normed = normed.astype(jnp.bfloat16)
    ep_count = lax.axis_size("ep")
    tp_count = lax.axis_size("tp")
    experts = ep_count * tp_count
    capacity = 2 * row_count * top_count // experts
    copies = row_count * top_count
    flat_routes = routes.reshape(copies)
    onehot = (flat_routes[:, None] == jnp.arange(experts, dtype=jnp.int32)[None, :]).astype(
        jnp.int32
    )
    slot_index = jnp.sum((jnp.cumsum(onehot, axis=0) - onehot) * onehot, axis=1)
    target = flat_routes * capacity + slot_index
    source_row = jnp.arange(copies, dtype=jnp.int32) // top_count
    slot_table = jnp.full((experts * capacity,), row_count, jnp.int32).at[target].set(source_row)
    padded = jnp.concatenate([normed, jnp.zeros((1, model_width), jnp.bfloat16)], axis=0)
    outgoing = padded[slot_table].reshape(experts, capacity, model_width)
    results = expert_rows(
        lax.all_to_all(outgoing, ("ep", "tp"), split_axis=0, concat_axis=0, tiled=True),
        gate_weight,
        up_weight,
        down_weight,
    )
    returned = lax.all_to_all(results, ("ep", "tp"), split_axis=0, concat_axis=0, tiled=True)
    returned = returned.reshape(experts * capacity, model_width)
    picked = returned[target].astype(jnp.float32) * route_weight.reshape(copies)[:, None]
    return picked.reshape(row_count, top_count, model_width).sum(axis=1).astype(jnp.bfloat16)


def on_device(
    pool_input,
    pool_map,
    pool_scale,
    out_weight,
    expert_input,
    norm_gain,
    routes,
    route_weight,
    gate_weight,
    up_weight,
    down_weight,
):
    pool_output = pool_half(pool_input, pool_map, pool_scale, out_weight)
    expert_output = expert_half(
        expert_input, norm_gain, routes, route_weight, gate_weight, up_weight, down_weight
    )
    return (pool_output, expert_output)


def solution(mesh):
    return jax.shard_map(
        on_device,
        mesh=mesh,
        in_specs=(
            P(("grp", "ep"), "tp"),
            P(),
            P(),
            P(None, "tp"),
            P(("grp", "ep", "tp"), None),
            P(),
            P(("grp", "ep", "tp"), None),
            P(("grp", "ep", "tp"), None),
            P(("ep", "tp"), None, None),
            P(("ep", "tp"), None, None),
            P(("ep", "tp"), None, None),
        ),
        out_specs=(P(("grp", "ep"), "tp"), P(("grp", "ep", "tp"), None)),
        check_vma=False,
    )
```

profile of v0, /device:TPU:0, one launch (start us, length us, event | category | flops | bytes accessed | tf_op | source)
XLA Modules:
  0.0 192.7 jit_solution(14643236694304669269)
XLA Ops:
  7.2 0.0 copy-start
  7.2 0.9 copy.19
  8.1 0.1 eq.31
  8.3 0.1 eq.27
  8.4 0.7 broadcast_multiply_fusion
  9.1 0.6 reduce-window.6
  9.7 0.2 slice_reduce_fusion
  9.9 0.1 copy.18
  10.0 0.1 mul.83
  10.2 0.1 fusion.43
  10.3 1.4 scatter_custom_fusion
  11.7 1.2 fusion.11
  12.9 1.2 fusion.13
  14.2 3.3 %gather_fusion = bf16[512,2048]{1,0:T(8,128)(2,1)} fusion(bf16[129,2048]{1,0:T(8,128)(2,1)S(1)} %concatenate.7, s32[1024]{0:T(1024)S(1)} %pad_clamp_fusion.1), kind=kCustom, calls=%fused_computation | custom fusion | bytes 4196352 | tf_op jit(solution)/shard_map/gather | solution.py:86
  17.6 7.5 %all-to-all-start = ((bf16[16,32,2048]{2,1,0:T(8,128)(2,1)}), bf16[16,32,2048]{2,1,0:T(8,128)(2,1)}, u32[]{:S(2)}, u32[]{:S(2)}) async-start(bf16[16,32,2048]{2,1,0:T(8,128)(2,1)} %bitcast.57), calls=%async_computation | async-start | bytes 4194304 | tf_op jit(solution)/shard_map/all_to_all | solution.py:88
  25.0 0.7 slice.58
  25.8 2.2 %collective-permute-start = (bf16[16,256]{1,0:T(8,128)(2,1)S(1)}, bf16[16,256]{1,0:T(8,128)(2,1)S(1)}, u32[]{:S(2)}, u32[]{:S(2)}) collective-permute-start(bf16[16,256]{1,0:T(8,128)(2,1)S(1)} %slice.58), channel_id=1, source_target_pairs={{0,4},{4,8},{8,12},{1,5},{5,9},{9,13},{2,6},{6,10},{10,14},{3,7},{... | collective-permute-start | bytes 24584 | tf_op jit(solution)/shard_map/ppermute | solution.py:13
  28.2 0.8 dynamic_slice.7
  29.0 0.0 collective-permute-done
  29.0 1.1 maximum_convert_fusion
  30.1 44.3 %all-to-all-done = bf16[16,32,2048]{2,1,0:T(8,128)(2,1)} async-done(((bf16[16,32,2048]{2,1,0:T(8,128)(2,1)}), bf16[16,32,2048]{2,1,0:T(8,128)(2,1)}, u32[]{:S(2)}, u32[]{:S(2)}) %all-to-all-start) | async-done | bytes 2097184 | tf_op jit(solution)/shard_map/all_to_all | solution.py:88
  74.4 4.4 %fusion.3 = f32[512,512]{1,0:T(8,128)} fusion(bf16[512,2048]{1,0:T(8,128)(2,1)} %bitcast.6, bf16[1,2048,512]{2,1,0:T(8,128)(2,1)} %param.19), kind=kOutput, calls=%fused_computation.7 | convolution fusion | flops 1073741824 | bytes 5242880 | tf_op jit(solution)/shard_map/dot_general | solution.py:19
  78.9 0.0 copy-done
  78.9 6.3 %convolution_convert_fusion = bf16[512,2048]{1,0:T(8,128)(2,1)} fusion(bf16[1,512,2048]{2,1,0:T(8,128)(2,1)S(1)} %copy-done, bf16[512,2048]{1,0:T(8,128)(2,1)} %bitcast.6, bf16[1,2048,512]{2,1,0:T(8,128)(2,1)} %param.20, f32[512,512]{1,0:T(8,128)} %fusion.3), kind=kOutput, calls=%fused_computation.3 | convolution fusion | flops 2150105088 | bytes 9437184 | tf_op jit(solution)/shard_map/dot_general | solution.py:22
  85.1 4.4 %all-to-all-start.1 = ((bf16[16,32,2048]{2,1,0:T(8,128)(2,1)}), bf16[16,32,2048]{2,1,0:T(8,128)(2,1)}, u32[]{:S(2)}, u32[]{:S(2)}) async-start(bf16[16,32,2048]{2,1,0:T(8,128)(2,1)} %bitcast.58), calls=%async_computation.1 | async-start | bytes 4194304 | tf_op jit(solution)/shard_map/all_to_all | solution.py:93
  89.6 0.2 all-gather.2.cloned.1.call-start
  89.8 3.8 %fusion.35 = f32[2,128,1024]{2,1,0:T(8,128)S(1)} fusion(bf16[8,128,128]{2,1,0:T(8,128)(2,1)} %param.12, s32[]{:T(128)S(6)} %select_n.92, s32[256]{0:T(256)S(1)} %fusion.46, s32[1024]{0:T(1024)S(1)} %add_add_fusion, f32[1040,256]{1,0:T(8,128)S(1)} %maximum_convert_fusion, pred[256]{0:T(512)(128)(4,1)S(1)} %get-tuple-element.2, ...), kind=kOutput, calls=%fused_computation.54 | convolution fusion | flops 76546048 | bytes 17904644 | tf_op jit(solution)/shard_map/rgc,gcd->rgd/dot_general | solution.py:47
  93.7 0.0 copy-start.1
  93.7 0.0 copy-start.2
  93.7 0.9 fusion.31
  94.6 0.0 all-gather.2.cloned.1.call-update
  94.6 0.0 copy-done.1
  94.6 0.1 copy.22
  94.8 75.0 %all-gather.2.cloned.1.call-done = bf16[1024,1024]{0,1:T(8,128)(2,1)} async-done(((bf16[1024,256]{0,1:T(8,128)(2,1)}), bf16[1024,1024]{0,1:T(8,128)(2,1)}) %all-gather.2.cloned.1.call-update) | async-done | bytes 2097168 | tf_op jit(solution)/shard_map/all_gather | solution.py:55
  169.8 0.0 copy-done.2
  169.8 3.9 %convolution_convert_fusion.1 = bf16[1024,512]{1,0:T(8,128)(2,1)} fusion(bf16[1024,1024]{0,1:T(8,128)(2,1)} %all-gather.2.cloned.1.call-done, bf16[1024,512]{1,0:T(8,128)(2,1)S(1)} %copy-done.2), kind=kOutput, calls=%fused_computation.10 | convolution fusion | flops 1074266112 | bytes 4194304 | tf_op jit(solution)/shard_map/dot_general | solution.py:54
  173.6 0.0 all-to-all-done.1
  173.6 4.2 %gather_fusion.1 = bf16[256,2048]{1,0:T(8,128)(2,1)S(1)} fusion(bf16[512,2048]{1,0:T(8,128)(2,1)} %bitcast.11, s32[1024]{0:T(1024)S(1)} %pad_clamp_fusion), kind=kCustom, calls=%fused_computation.1 | custom fusion | bytes 2098176 | tf_op jit(solution)/shard_map/gather | solution.py:95
  177.9 2.4 %reshape.127 = f32[128,2,2048]{2,1,0:T(2,128)} reshape(bf16[256,2048]{1,0:T(8,128)(2,1)S(1)} %gather_fusion.1) | data formatting | bytes 3145728 | tf_op jit(solution)/shard_map/convert_element_type | solution.py:95
  180.2 5.6 %multiply_reduce_fusion = bf16[128,2048]{1,0:T(8,128)(2,1)} fusion(f32[128,2,2048]{2,1,0:T(2,128)} %reshape.127, f32[128,2]{1,0:T(8,128)S(1)} %copy.22), kind=kLoop, calls=%fused_computation.9 | loop fusion | flops 786432 | bytes 2622464 | tf_op jit(solution)/shard_map/reduce_sum | solution.py:96
  (20 shorter events, 0.3 us)
Async XLA Ops:
  7.2 71.7 %copy-start = (bf16[1,512,2048]{2,1,0:T(8,128)(2,1)S(1)}, bf16[1,512,2048]{2,1,0:T(8,128)(2,1)}, u32[]{:S(2)}) copy-start(bf16[1,512,2048]{2,1,0:T(8,128)(2,1)} %param.21) | copy-start | bytes 6291460
  17.6 56.8 %all-to-all-start = ((bf16[16,32,2048]{2,1,0:T(8,128)(2,1)}), bf16[16,32,2048]{2,1,0:T(8,128)(2,1)}, u32[]{:S(2)}, u32[]{:S(2)}) async-start(bf16[16,32,2048]{2,1,0:T(8,128)(2,1)} %bitcast.57), calls=%async_computation | async-start | bytes 4194304 | tf_op jit(solution)/shard_map/all_to_all | solution.py:88
  25.8 3.2 %collective-permute-start = (bf16[16,256]{1,0:T(8,128)(2,1)S(1)}, bf16[16,256]{1,0:T(8,128)(2,1)S(1)}, u32[]{:S(2)}, u32[]{:S(2)}) collective-permute-start(bf16[16,256]{1,0:T(8,128)(2,1)S(1)} %slice.58), channel_id=1, source_target_pairs={{0,4},{4,8},{8,12},{1,5},{5,9},{9,13},{2,6},{6,10},{10,14},{3,7},{... | collective-permute-start | bytes 24584 | tf_op jit(solution)/shard_map/ppermute | solution.py:13
  85.1 88.5 %all-to-all-start.1 = ((bf16[16,32,2048]{2,1,0:T(8,128)(2,1)}), bf16[16,32,2048]{2,1,0:T(8,128)(2,1)}, u32[]{:S(2)}, u32[]{:S(2)}) async-start(bf16[16,32,2048]{2,1,0:T(8,128)(2,1)} %bitcast.58), calls=%async_computation.1 | async-start | bytes 4194304 | tf_op jit(solution)/shard_map/all_to_all | solution.py:93
  89.6 80.2 %all-gather.2.cloned.1.call-start = ((), (), s32[]{:S(2)}) async-start(), calls=%async_computation.2 | async-start | bytes 2621440 | tf_op jit(solution)/shard_map/all_gather | solution.py:55
  93.7 1.0 copy-start.1
  93.7 76.1 %copy-start.2 = (bf16[1024,512]{1,0:T(8,128)(2,1)S(1)}, bf16[1024,512]{1,0:T(8,128)(2,1)}, u32[]{:S(2)}) copy-start(bf16[1024,512]{1,0:T(8,128)(2,1)} %param.14) | copy-start | bytes 3145732
Sparse Core Ops, SparseCore 0:
  94.7 74.9 all-gather.1
where the time goes:
time: 193 us
  waiting for transfers between devices  119 us (62%)
  matrix products  18.4 us (10%)
  local copies, waits for them, and re-layouts  14.6 us (8%)
  starting transfers between devices  14.4 us (7%)
  between operations  14.2 us (7%)
  other arithmetic  11.7 us (6%)
    all_gather x1, waiting for transfers between devices, pool_half(): lax.all_gather(mapped, 'tp', axis=1, tiled=True)  75 us
    all_to_all x1, waiting for transfers between devices, expert_half(): lax.all_to_all(outgoing, ('ep', 'tp'), split_axis=0, concat_axis=0, tiled...  44.3 us
    all_to_all x1, starting transfers between devices, expert_half(): lax.all_to_all(outgoing, ('ep', 'tp'), split_axis=0, concat_axis=0, tiled...  7.46 us
    dot_general x1, matrix products, expert_rows(): jnp.dot(hidden, down_weight[0], preferred_element_type=jnp.float32)  6.28 us
    reduce_sum x1, other arithmetic, expert_half(): picked.reshape(row_count, top_count, model_width).sum(axis=1)  5.59 us
    dot_general x1, matrix products, expert_rows(): jnp.dot(flat_rows, gate_weight[0], preferred_element_type=jnp.float32)  4.44 us
    all_to_all x1, starting transfers between devices, expert_half(): lax.all_to_all(results, ('ep', 'tp'), split_axis=0, concat_axis=0, tiled=...  4.44 us
    gather x1, local copies, waits for them, and re-layouts, expert_half(): returned[target].astype(jnp.float32) * route_weight.reshape(copies)[:, None]  4.22 us
  transfers between devices with their start and end apart: 4, of which 2 were waited for; matrix products, arithmetic and copies ran while one was open for 6% of the time, Pallas kernels for 0%

commit v1 on v0

v1 whole, which is shorter than its diff:
```python
import jax
import jax.numpy as jnp
from jax import lax
from jax.sharding import PartitionSpec as P

epsilon = 1e-06
halo_depth = 16
f32 = jnp.float32
bf16 = jnp.bfloat16


def moved(block, axis, by, keep):
    size = lax.axis_size(axis)
    pairs = [(i, i + by) for i in range(size) if 0 <= i + by < size and keep(i)]
    return lax.ppermute(block, axis, pairs)


def gather_line(block, axis):
    size = lax.axis_size(axis)
    from_left, from_right = [block], [block]
    for step in range(1, size):
        from_left.append(moved(from_left[-1], axis, 1, lambda i: i >= step - 1))
        from_right.append(moved(from_right[-1], axis, -1, lambda i: i <= size - step))
    blocks = [block]
    own = lax.axis_index(axis)
    for m in range(1, size):
        blocks.append(jnp.where(own + m < size, from_right[m], from_left[size - m]))
    return blocks, (from_left[-1], from_right[-1])


def scatter_line(partials, axis):
    size = lax.axis_size(axis)
    right, left = None, None
    for step in range(1, size):
        to_right, to_left = partials[size - step], partials[step]
        if step > 1:
            to_right, to_left = to_right + right.astype(f32), to_left + left.astype(f32)
        right = moved(to_right.astype(bf16), axis, 1, lambda i: i <= step - 1)
        left = moved(to_left.astype(bf16), axis, -1, lambda i: i >= size - step)
    total = partials[0]
    if size > 1:
        total = total + right.astype(f32) + left.astype(f32)
    return total


def expert_rows(received, gate_weight, up_weight, down_weight):
    shape_in = received.shape
    flat_rows = received.reshape(-1, shape_in[-1])
    gate_part = jnp.dot(flat_rows, gate_weight[0], preferred_element_type=f32)
    up_part = jnp.dot(flat_rows, up_weight[0], preferred_element_type=f32)
    hidden = (jax.nn.silu(gate_part) * up_part).astype(bf16)
    result = jnp.dot(hidden, down_weight[0], preferred_element_type=f32).astype(bf16)
    return result.reshape(shape_in)


def pool_mapped(pool_input, pool_map, pool_scale):
    row_count, width_local = pool_input.shape
    group_dim = pool_map.shape[1]
    groups_local = width_local // group_dim
    last_rows = pool_input[row_count - halo_depth :]
    earlier_rows = moved(last_rows, "ep", 1, lambda i: True)
    extended = jnp.concatenate([earlier_rows, pool_input], axis=0).astype(f32)
    first_group = lax.axis_index("tp") * groups_local
    group_ids = first_group + jnp.arange(width_local, dtype=jnp.int32) // group_dim
    window = jnp.left_shift(jnp.int32(2), group_ids % 4)
    summed = jnp.zeros((row_count, width_local), f32)
    for offset in range(halo_depth):
        shifted = extended[halo_depth - offset : halo_depth - offset + row_count]
        summed = summed + jnp.where(offset < window, shifted, 0.0)
    positions = lax.axis_index("ep") * row_count + jnp.arange(row_count, dtype=jnp.int32)
    counted = jnp.minimum(positions[:, None] + 1, window[None, :]).astype(f32)
    pooled = (summed / counted - extended[halo_depth:]).astype(bf16)
    maps_local = lax.dynamic_slice_in_dim(pool_map, first_group, groups_local, 0)
    scales_local = lax.dynamic_slice_in_dim(pool_scale, first_group * group_dim, width_local, 0)
    mapped = jnp.einsum(
        "rgc,gcd->rgd",
        pooled.reshape(row_count, groups_local, group_dim),
        maps_local,
        preferred_element_type=f32,
    )
    return (mapped.reshape(row_count, width_local) * scales_local).astype(bf16)


def pool_project(blocks, out_weight):
    size = len(blocks)
    depth = blocks[0].shape[1]
    own = lax.axis_index("tp")
    total = None
    for m in range(size):
        rows = lax.dynamic_slice_in_dim(out_weight, (own + m) % size * depth, depth, 0)
        product = jnp.dot(blocks[m], rows, preferred_element_type=f32)
        total = product if total is None else total + product
    return total.astype(bf16)


def on_device(
    pool_input,
    pool_map,
    pool_scale,
    out_weight,
    expert_input,
    norm_gain,
    routes,
    route_weight,
    gate_weight,
    up_weight,
    down_weight,
):
    row_count, model_width = expert_input.shape
    top_count = routes.shape[1]
    ep_count = lax.axis_size("ep")
    tp_count = lax.axis_size("tp")
    capacity = 2 * row_count * top_count // (ep_count * tp_count)
    own = lax.axis_index("tp")

    widened = expert_input.astype(f32)
    normed = (
        widened
        * lax.rsqrt(jnp.mean(widened * widened, axis=1, keepdims=True) + epsilon)
        * norm_gain
    ).astype(bf16)
    tokens, last_tokens = gather_line(normed, "tp")

    facts = jnp.concatenate([routes.astype(f32), route_weight], axis=1).T
    facts = lax.all_gather(facts, "tp", axis=0, tiled=False)
    facts = jnp.concatenate([facts, facts], axis=0)
    facts = lax.dynamic_slice_in_dim(facts, own, tp_count, 0)
    routes_all = facts[:, :top_count].astype(jnp.int32)
    weights_all = facts[:, top_count:]
    named = jnp.arange(ep_count, dtype=jnp.int32) * tp_count + own
    match = (routes_all[:, :, None, :] == named[None, None, :, None]).astype(f32)
    chosen = match.sum(axis=1)
    scale = (match * weights_all[:, :, None, :]).sum(axis=1)
    earlier = (
        jnp.arange(row_count, dtype=jnp.int32)[:, None]
        < jnp.arange(row_count, dtype=jnp.int32)[None, :]
    ).astype(bf16)
    rank = jnp.dot(
        chosen.reshape(-1, row_count).astype(bf16), earlier, preferred_element_type=f32
    ).reshape(tp_count, ep_count, row_count).astype(jnp.int32)
    slots = jnp.arange(capacity, dtype=jnp.int32)
    taken = (rank[:, :, None, :] == slots[None, None, :, None]) & (chosen[:, :, None, :] > 0)

    groups = [
        [m for m in range(tp_count) if m not in (1, tp_count - 1)],
        sorted({1, tp_count - 1} & set(range(1, tp_count))),
    ]
    partials = [None] * tp_count
    for group in groups:
        if not group:
            continue
        count = len(group)
        taken_here = jnp.stack([taken[m] for m in group], axis=1)
        scale_here = jnp.stack([scale[m] for m in group], axis=1)
        same = jnp.eye(count, dtype=bool)[None, :, None, :, None]
        select = (taken_here[:, :, :, None, :] & same).astype(bf16)
        rows = ep_count * count * capacity
        outgoing = jnp.dot(
            select.reshape(rows, count * row_count),
            jnp.concatenate([tokens[m] for m in group], axis=0),
            preferred_element_type=f32,
        ).astype(bf16)
        received = lax.all_to_all(
            outgoing.reshape(ep_count, count * capacity, model_width), "ep", 0, 0, tiled=True
        )
        results = expert_rows(received, gate_weight, up_weight, down_weight)
        returned = lax.all_to_all(results, "ep", 0, 0, tiled=True).reshape(rows, model_width)
        for place, m in enumerate(group):
            mine = taken_here & (jnp.arange(count) == place)[None, :, None, None]
            weighted = jnp.where(mine, scale_here[:, :, None, :], 0.0).reshape(rows, row_count).T
            upper = weighted.astype(bf16)
            lower = (weighted - upper.astype(f32)).astype(bf16)
            partials[m] = jnp.dot(upper, returned, preferred_element_type=f32) + jnp.dot(
                lower, returned, preferred_element_type=f32
            )

    mapped = pool_mapped(pool_input, pool_map, pool_scale)
    mapped, last_tokens = lax.optimization_barrier((mapped, last_tokens))
    pool_blocks, unused = gather_line(mapped, "tp")
    pool_output = pool_project(pool_blocks, out_weight)
    expert_output = scatter_line(partials, "tp").astype(bf16)
    return (pool_output, expert_output)


def solution(mesh):
    return jax.shard_map(
        on_device,
        mesh=mesh,
        in_specs=(
            P(("grp", "ep"), "tp"),
            P(),
            P(),
            P(None, "tp"),
            P(("grp", "ep", "tp"), None),
            P(),
            P(("grp", "ep", "tp"), None),
            P(("grp", "ep", "tp"), None),
            P(("ep", "tp"), None, None),
            P(("ep", "tp"), None, None),
            P(("ep", "tp"), None, None),
        ),
        out_specs=(P(("grp", "ep"), "tp"), P(("grp", "ep", "tp"), None)),
        check_vma=False,
    )
```

time: 193 us -> 203 us (1.052)
  starting transfers between devices: 14.4 us -> 53.9 us
  waiting for transfers between devices: 119 us -> 80 us
  matrix products: 18.4 us -> 36.8 us
  between operations: 14.2 us -> 1.2 us
  blocking collectives: 0 us -> 12 us
  local copies, waits for them, and re-layouts: 14.6 us -> 3.82 us
  other arithmetic: 11.7 us -> 14.2 us
    all_gather x1 -> x0, waiting for transfers between devices: 75 us -> none  [pool_half(): lax.all_gather(mapped, 'tp', axis=1, tiled=True)]
    ppermute x1 -> x19, waiting for transfers between devices: 0.01 us -> 56.4 us  [moved(): return lax.ppermute(block, axis, pairs)]
    ppermute x1 -> x19, starting transfers between devices: 2.25 us -> 39.1 us  [moved(): return lax.ppermute(block, axis, pairs)]
    all_to_all x2 -> x4, waiting for transfers between devices: 44.3 us -> 23.6 us  [the longest x2 12 us: on_device(): lax.all_to_all(outgoing.reshape(ep_count, count * capacity, model_width),...]
    dot_general x4 -> x20, matrix products: 18.4 us -> 36.8 us  [the longest x2 8.63 us: expert_rows(): jnp.dot(hidden, down_weight[0], preferred_element_type=f32).astype(bf16)]
    all_gather x0 -> x1, blocking collectives: none -> 12 us  [on_device(): facts = lax.all_gather(facts, 'tp', axis=0, tiled=False)]
    gather x2 -> x0, local copies, waits for them, and re-layouts: 7.57 us -> none  [the longest x1 4.22 us: expert_half(): returned[target].astype(jnp.float32) * route_weight.reshape(copies)[:, None]]
    reduce_sum x3 -> x2, other arithmetic: 6.9 us -> 1.47 us  [the longest x1 1.39 us: on_device(): jnp.mean(widened * widened, axis=1, keepdims=True) + epsilon]
  transfers between devices with their start and end apart: 4 -> 23, of which waited for: 2 -> 11; matrix products, arithmetic and copies ran while one was open for 6% -> 23% of each run, Pallas kernels for 0% -> 0%
where the time goes in v1:
time: 203 us; the launch traced here: 202 us
  waiting for transfers between devices  80 us (39%)
  starting transfers between devices  53.9 us (27%)
  matrix products  36.8 us (18%)
  other arithmetic  14.2 us (7%)
  blocking collectives  12 us (6%)
  local copies, waits for them, and re-layouts  3.82 us (2%)
    ppermute x19, waiting for transfers between devices, moved(): return lax.ppermute(block, axis, pairs)  56.4 us
    ppermute x19, starting transfers between devices, moved(): return lax.ppermute(block, axis, pairs)  39.1 us
    all_gather x1, blocking collectives, on_device(): facts = lax.all_gather(facts, 'tp', axis=0, tiled=False)  12 us
    all_to_all x2, waiting for transfers between devices, on_device(): lax.all_to_all(outgoing.reshape(ep_count, count * capacity, model_width),...  12 us
    all_to_all x2, waiting for transfers between devices, on_device(): lax.all_to_all(results, 'ep', 0, 0, tiled=True).reshape(rows, model_width)  11.7 us
    dot_general x2, matrix products, expert_rows(): jnp.dot(hidden, down_weight[0], preferred_element_type=f32).astype(bf16)  8.63 us
    all_to_all x2, starting transfers between devices, on_device(): lax.all_to_all(outgoing.reshape(ep_count, count * capacity, model_width),...  7.76 us
    all_to_all x2, starting transfers between devices, on_device(): lax.all_to_all(results, 'ep', 0, 0, tiled=True).reshape(rows, model_width)  7.03 us
  transfers between devices with their start and end apart: 23, of which 11 were waited for; matrix products, arithmetic and copies ran while one was open for 23% of the time, Pallas kernels for 0%

profile of v1, /device:TPU:0, one launch (start us, length us, event | category | flops | bytes accessed | tf_op | source)
XLA Modules:
  0.0 201.9 jit_solution(14717826679928241467)
XLA Ops:
  0.7 1.4 fusion.22
  2.1 2.0 %fusion.24 = bf16[128,2048]{1,0:T(8,128)(2,1)} fusion(bf16[128,2048]{1,0:T(8,128)(2,1)} %param.15, f32[2048]{0:T(1024)} %param.16, f32[128]{0:T(128)S(1)} %add_rsqrt_fusion), kind=kLoop, calls=%fused_computation.28 | loop fusion | flops 1048576 | bytes 1057280 | tf_op jit(solution)/shard_map/convert_element_type | solution.py:121
  4.1 1.3 collective-permute-start.4
  5.4 6.4 %collective-permute-start.1 = (bf16[128,2048]{1,0:T(8,128)(2,1)}, bf16[128,2048]{1,0:T(8,128)(2,1)}, u32[]{:S(2)}, u32[]{:S(2)}) collective-permute-start(bf16[128,2048]{1,0:T(8,128)(2,1)} %fusion.24), channel_id=1, source_target_pairs={{0,1},{1,2},{2,3},{4,5},{5,6},{6,7},{8,9},{9,10},{10,11},{12,13},{... | collective-permute-start | bytes 1572872 | tf_op jit(solution)/shard_map/ppermute | solution.py:15
  12.5 1.4 collective-permute-start
  18.9 12.0 %all-gather.1 = f32[4,4,128]{2,1,0:T(4,128)S(1)} all-gather(f32[1,4,128]{2,1,0:T(4,128)S(1)} %maximum_bitcast_fusion), channel_id=2, replica_groups=mesh['grp'=2,'ep'=4,'tp'=4] {'tp'}, dimensions={0}, use_global_device_ids=true | all-gather | bytes 10240 | tf_op jit(solution)/shard_map/all_gather | solution.py:125
  32.3 1.3 collective-permute-start.5
  33.6 1.5 collective-permute-start.2
  37.4 10.7 %collective-permute-done.5 = bf16[128,2048]{1,0:T(8,128)(2,1)} collective-permute-done((bf16[128,2048]{1,0:T(8,128)(2,1)S(1)}, bf16[128,2048]{1,0:T(8,128)(2,1)}, u32[]{:S(2)}, u32[]{:S(2)}) %collective-permute-start.5) | collective-permute-done | bytes 524320 | tf_op jit(solution)/shard_map/ppermute | solution.py:15
  48.0 1.3 collective-permute-start.6
  50.1 3.9 %fusion.54 = f32[2,128,1024]{2,1,0:T(8,128)S(1)} fusion(bf16[8,128,128]{2,1,0:T(8,128)(2,1)} %param.12, s32[]{:T(128)S(6)} %select_n.165, s32[256]{0:T(256)S(1)} %fusion.104, s32[1024]{0:T(1024)S(1)} %add_add_fusion, f32[1040,256]{1,0:T(8,128)S(1)} %maximum_convert_fusion, pred[256]{0:T(512)(128)(4,1)} %get-tuple-element.36, ...), kind=kOutput, calls=%fused_computation.76 | convolution fusion | flops 76546048 | bytes 17904644 | tf_op jit(solution)/shard_map/rgc,gcd->rgd/dot_general | solution.py:75
  54.0 9.0 %collective-permute-done.6 = bf16[128,2048]{1,0:T(8,128)(2,1)S(1)} collective-permute-done((bf16[128,2048]{1,0:T(8,128)(2,1)}, bf16[128,2048]{1,0:T(8,128)(2,1)S(1)}, u32[]{:S(2)}, u32[]{:S(2)}) %collective-permute-start.6) | collective-permute-done | bytes 524320 | tf_op jit(solution)/shard_map/ppermute | solution.py:15
  63.1 1.4 convolution_convert_fusion.2
  64.6 4.2 %all-to-all-start.2 = ((bf16[4,64,2048]{2,1,0:T(8,128)(2,1)}), bf16[4,64,2048]{2,1,0:T(8,128)(2,1)}, u32[]{:S(2)}, u32[]{:S(2)}) async-start(bf16[4,64,2048]{2,1,0:T(8,128)(2,1)} %bitcast.209), calls=%async_computation.2 | async-start | bytes 2097152 | tf_op jit(solution)/shard_map/all_to_all | solution.py:163
  70.9 2.5 %convolution_convert_fusion.3 = bf16[256,2048]{1,0:T(8,128)(2,1)} fusion(bf16[128,2048]{1,0:T(8,128)(2,1)S(1)} %broadcast_select_fusion.2, bf16[128,2048]{1,0:T(8,128)(2,1)} %fusion.24, pred[32,8,2,128]{3,2,1,0:T(4,128)(4,1)S(1)} %bitcast.213), kind=kOutput, calls=%fused_computation.3 | convolution fusion | flops 271056896 | bytes 2162688 | tf_op jit(solution)/shard_map/dot_general | solution.py:158
  73.3 3.4 %collective-permute-start.8 = (bf16[1024,256]{0,1:T(8,128)(2,1)}, bf16[1024,256]{0,1:T(8,128)(2,1)}, u32[]{:S(2)}, u32[]{:S(2)}) collective-permute-start(bf16[1024,256]{0,1:T(8,128)(2,1)} %fusion.48), channel_id=1, source_target_pairs={{0,1},{1,2},{2,3},{4,5},{5,6},{6,7},{8,9},{9,10},{10,11},{12,13},{... | collective-permute-start | bytes 1572872 | tf_op jit(solution)/shard_map/ppermute | solution.py:15
  76.7 1.3 collective-permute-start.7
  78.0 5.3 %all-to-all-done.2 = bf16[4,64,2048]{2,1,0:T(8,128)(2,1)} async-done(((bf16[4,64,2048]{2,1,0:T(8,128)(2,1)}), bf16[4,64,2048]{2,1,0:T(8,128)(2,1)}, u32[]{:S(2)}, u32[]{:S(2)}) %all-to-all-start.2) | async-done | bytes 1048608 | tf_op jit(solution)/shard_map/all_to_all | solution.py:163
  83.3 3.5 %all-to-all-start = ((bf16[4,64,2048]{2,1,0:T(8,128)(2,1)}), bf16[4,64,2048]{2,1,0:T(8,128)(2,1)S(1)}, u32[]{:S(2)}, u32[]{:S(2)}) async-start(bf16[4,64,2048]{2,1,0:T(8,128)(2,1)} %bitcast.13), calls=%async_computation | async-start | bytes 2097152 | tf_op jit(solution)/shard_map/all_to_all | solution.py:163
  86.8 3.4 %fusion.6 = f32[256,512]{1,0:T(8,128)} fusion(bf16[256,2048]{1,0:T(8,128)(2,1)} %bitcast.28, bf16[1,2048,512]{2,1,0:T(8,128)(2,1)} %param.19), kind=kOutput, calls=%fused_computation.14 | convolution fusion | flops 536870912 | bytes 3670016 | tf_op jit(solution)/shard_map/dot_general | solution.py:49
  90.3 4.3 %convolution_convert_fusion = bf16[256,2048]{1,0:T(8,128)(2,1)} fusion(bf16[1,512,2048]{2,1,0:T(8,128)(2,1)S(1)} %copy-done, bf16[256,2048]{1,0:T(8,128)(2,1)} %bitcast.28, bf16[1,2048,512]{2,1,0:T(8,128)(2,1)} %param.20, f32[256,512]{1,0:T(8,128)} %fusion.6), kind=kOutput, calls=%fused_computation | convolution fusion | flops 1075052544 | bytes 6815744 | tf_op jit(solution)/shard_map/dot_general | solution.py:52
  94.6 6.7 %all-to-all-done = bf16[4,64,2048]{2,1,0:T(8,128)(2,1)S(1)} async-done(((bf16[4,64,2048]{2,1,0:T(8,128)(2,1)}), bf16[4,64,2048]{2,1,0:T(8,128)(2,1)S(1)}, u32[]{:S(2)}, u32[]{:S(2)}) %all-to-all-start) | async-done | bytes 1048608 | tf_op jit(solution)/shard_map/all_to_all | solution.py:163
  102.2 3.5 %all-to-all-start.3 = ((bf16[4,64,2048]{2,1,0:T(8,128)(2,1)}), bf16[4,64,2048]{2,1,0:T(8,128)(2,1)S(1)}, u32[]{:S(2)}, u32[]{:S(2)}) async-start(bf16[4,64,2048]{2,1,0:T(8,128)(2,1)} %bitcast.212), calls=%async_computation.3 | async-start | bytes 2097152 | tf_op jit(solution)/shard_map/all_to_all | solution.py:167
  105.7 3.4 %fusion.8 = f32[256,512]{1,0:T(8,128)} fusion(bf16[256,2048]{1,0:T(8,128)(2,1)} %bitcast.210, bf16[1,2048,512]{2,1,0:T(8,128)(2,1)} %param.19), kind=kOutput, calls=%fused_computation.16 | convolution fusion | flops 536870912 | bytes 3670016 | tf_op jit(solution)/shard_map/dot_general | solution.py:49
  109.2 4.3 %convolution_convert_fusion.1 = bf16[256,2048]{1,0:T(8,128)(2,1)} fusion(bf16[1,512,2048]{2,1,0:T(8,128)(2,1)S(1)} %copy-done, bf16[256,2048]{1,0:T(8,128)(2,1)} %bitcast.211, bf16[1,2048,512]{2,1,0:T(8,128)(2,1)} %param.20, f32[256,512]{1,0:T(8,128)} %fusion.8), kind=kOutput, calls=%fused_computation.1 | convolution fusion | flops 1075052544 | bytes 6815744 | tf_op jit(solution)/shard_map/dot_general | solution.py:52
  113.5 6.6 %all-to-all-done.3 = bf16[4,64,2048]{2,1,0:T(8,128)(2,1)S(1)} async-done(((bf16[4,64,2048]{2,1,0:T(8,128)(2,1)}), bf16[4,64,2048]{2,1,0:T(8,128)(2,1)S(1)}, u32[]{:S(2)}, u32[]{:S(2)}) %all-to-all-start.3) | async-done | bytes 1048608 | tf_op jit(solution)/shard_map/all_to_all | solution.py:167
  121.1 3.5 %all-to-all-start.1 = ((bf16[4,64,2048]{2,1,0:T(8,128)(2,1)}), bf16[4,64,2048]{2,1,0:T(8,128)(2,1)S(1)}, u32[]{:S(2)}, u32[]{:S(2)}) async-start(bf16[4,64,2048]{2,1,0:T(8,128)(2,1)} %bitcast.208), calls=%async_computation.1 | async-start | bytes 2097152 | tf_op jit(solution)/shard_map/all_to_all | solution.py:167
  124.7 1.7 fusion.115
  126.3 1.5 fusion.111
  127.8 3.4 %collective-permute-start.13 = (bf16[128,2048]{1,0:T(8,128)(2,1)}, bf16[128,2048]{1,0:T(8,128)(2,1)}, u32[]{:S(2)}, u32[]{:S(2)}) collective-permute-start(bf16[128,2048]{1,0:T(8,128)(2,1)} %get-tuple-element.32), channel_id=1, source_target_pairs={{0,1},{4,5},{8,9},{12,13},{16,17},{20,21},{24,25},{28,29}} | collective-permute-start | bytes 1572872 | tf_op jit(solution)/shard_map/ppermute | solution.py:15
  131.3 1.5 collective-permute-start.9
  132.7 1.3 collective-permute-start.11
  134.0 5.0 %all-to-all-done.1 = bf16[4,64,2048]{2,1,0:T(8,128)(2,1)S(1)} async-done(((bf16[4,64,2048]{2,1,0:T(8,128)(2,1)}), bf16[4,64,2048]{2,1,0:T(8,128)(2,1)S(1)}, u32[]{:S(2)}, u32[]{:S(2)}) %all-to-all-start.1) | async-done | bytes 1048608 | tf_op jit(solution)/shard_map/all_to_all | solution.py:167
  139.0 1.2 fusion.114
  140.2 2.3 %collective-permute-done.13 = bf16[128,2048]{1,0:T(8,128)(2,1)} collective-permute-done((bf16[128,2048]{1,0:T(8,128)(2,1)}, bf16[128,2048]{1,0:T(8,128)(2,1)}, u32[]{:S(2)}, u32[]{:S(2)}) %collective-permute-start.13) | collective-permute-done | bytes 524320 | tf_op jit(solution)/shard_map/ppermute | solution.py:15
  142.5 1.5 add_convert_fusion.5
  144.0 4.6 %collective-permute-start.14 = (bf16[128,2048]{1,0:T(8,128)(2,1)S(1)}, bf16[128,2048]{1,0:T(8,128)(2,1)S(1)}, u32[]{:S(2)}, u32[]{:S(2)}) collective-permute-start(bf16[128,2048]{1,0:T(8,128)(2,1)S(1)} %get-tuple-element.34), channel_id=1, source_target_pairs={{0,1},{1,2},{4,5},{5,6},{8,9},{9,10},{12,13},{13,14},{16,17},{17,1... | collective-permute-start | bytes 1572872 | tf_op jit(solution)/shard_map/ppermute | solution.py:15
  149.3 10.0 %collective-permute-done.14 = bf16[128,2048]{1,0:T(8,128)(2,1)S(1)} collective-permute-done((bf16[128,2048]{1,0:T(8,128)(2,1)S(1)}, bf16[128,2048]{1,0:T(8,128)(2,1)S(1)}, u32[]{:S(2)}, u32[]{:S(2)}) %collective-permute-start.14) | collective-permute-done | bytes 524320 | tf_op jit(solution)/shard_map/ppermute | solution.py:15
  160.2 1.5 fusion.81
  162.4 1.3 collective-permute-start.12
  165.2 1.6 fusion.68
  166.9 5.2 %collective-permute-start.15 = (bf16[128,2048]{1,0:T(8,128)(2,1)S(1)}, bf16[128,2048]{1,0:T(8,128)(2,1)S(1)}, u32[]{:S(2)}, u32[]{:S(2)}) collective-permute-start(bf16[128,2048]{1,0:T(8,128)(2,1)S(1)} %get-tuple-element.6), channel_id=1, source_target_pairs={{0,1},{1,2},{2,3},{4,5},{5,6},{6,7},{8,9},{9,10},{10,11},{12,13},{... | collective-permute-start | bytes 1572872 | tf_op jit(solution)/shard_map/ppermute | solution.py:15
  172.2 1.3 collective-permute-start.18
  173.5 1.5 fusion.70
  175.1 2.1 %collective-permute-done.12 = bf16[1024,256]{0,1:T(8,128)(2,1)S(1)} collective-permute-done((bf16[1024,256]{0,1:T(8,128)(2,1)}, bf16[1024,256]{0,1:T(8,128)(2,1)S(1)}, u32[]{:S(2)}, u32[]{:S(2)}) %collective-permute-start.12) | collective-permute-done | bytes 524320 | tf_op jit(solution)/shard_map/ppermute | solution.py:15
  177.2 1.5 add_convert_fusion
  178.7 3.3 %collective-permute-done.15 = bf16[128,2048]{1,0:T(8,128)(2,1)S(1)} collective-permute-done((bf16[128,2048]{1,0:T(8,128)(2,1)S(1)}, bf16[128,2048]{1,0:T(8,128)(2,1)S(1)}, u32[]{:S(2)}, u32[]{:S(2)}) %collective-permute-start.15) | collective-permute-done | bytes 524320 | tf_op jit(solution)/shard_map/ppermute | solution.py:15
  181.9 19.0 %collective-permute-done.18 = bf16[128,2048]{1,0:T(8,128)(2,1)S(1)} collective-permute-done((bf16[128,2048]{1,0:T(8,128)(2,1)S(1)}, bf16[128,2048]{1,0:T(8,128)(2,1)S(1)}, u32[]{:S(2)}, u32[]{:S(2)}) %collective-permute-start.18) | collective-permute-done | bytes 524320 | tf_op jit(solution)/shard_map/ppermute | solution.py:15
  (95 shorter events, 18.9 us)
Async XLA Ops:
  0.6 89.6 %copy-start = (bf16[1,512,2048]{2,1,0:T(8,128)(2,1)S(1)}, bf16[1,512,2048]{2,1,0:T(8,128)(2,1)}, u32[]{:S(2)}) copy-start(bf16[1,512,2048]{2,1,0:T(8,128)(2,1)} %param.21) | copy-start | bytes 6291460
  0.6 36.6 %copy-start.7 = (bf16[1024,256]{1,0:T(8,128)(2,1)S(1)}, bf16[1024,256]{1,0:T(8,128)(2,1)}, u32[]{:S(2)}) copy-start(bf16[1024,256]{1,0:T(8,128)(2,1)} %param.11) | copy-start | bytes 1572868
  4.1 28.3 %collective-permute-start.4 = (bf16[128,2048]{1,0:T(8,128)(2,1)}, bf16[128,2048]{1,0:T(8,128)(2,1)S(1)}, u32[]{:S(2)}, u32[]{:S(2)}) collective-permute-start(bf16[128,2048]{1,0:T(8,128)(2,1)} %fusion.24), channel_id=1, source_target_pairs={{1,0},{2,1},{3,2},{5,4},{6,5},{7,6},{9,8},{10,9},{11,10},{13,12},{... | collective-permute-start | bytes 1572872 | tf_op jit(solution)/shard_map/ppermute | solution.py:15
  5.4 28.3 %collective-permute-start.1 = (bf16[128,2048]{1,0:T(8,128)(2,1)}, bf16[128,2048]{1,0:T(8,128)(2,1)}, u32[]{:S(2)}, u32[]{:S(2)}) collective-permute-start(bf16[128,2048]{1,0:T(8,128)(2,1)} %fusion.24), channel_id=1, source_target_pairs={{0,1},{1,2},{2,3},{4,5},{5,6},{6,7},{8,9},{9,10},{10,11},{12,13},{... | collective-permute-start | bytes 1572872 | tf_op jit(solution)/shard_map/ppermute | solution.py:15
  12.5 24.8 %collective-permute-start = (bf16[16,256]{1,0:T(8,128)(2,1)S(1)}, bf16[16,256]{1,0:T(8,128)(2,1)S(1)}, u32[]{:S(2)}, u32[]{:S(2)}) collective-permute-start(bf16[16,256]{1,0:T(8,128)(2,1)S(1)} %slice.82), channel_id=1, source_target_pairs={{0,4},{4,8},{8,12},{1,5},{5,9},{9,13},{2,6},{6,10},{10,14},{3,7},{... | collective-permute-start | bytes 24584 | tf_op jit(solution)/shard_map/ppermute | solution.py:15
  32.3 17.7 %copy-start.8 = (bf16[128,2048]{1,0:T(8,128)(2,1)}, bf16[128,2048]{1,0:T(8,128)(2,1)S(1)}, u32[]{:S(2)}) copy-start(bf16[128,2048]{1,0:T(8,128)(2,1)S(1)} %collective-permute-done.4) | copy-start | bytes 1572868
  32.3 15.7 %collective-permute-start.5 = (bf16[128,2048]{1,0:T(8,128)(2,1)S(1)}, bf16[128,2048]{1,0:T(8,128)(2,1)}, u32[]{:S(2)}, u32[]{:S(2)}) collective-permute-start(bf16[128,2048]{1,0:T(8,128)(2,1)S(1)} %collective-permute-done.4), channel_id=1, source_target_pairs={{1,0},{2,1},{5,4},{6,5},{9,8},{10,9},{13,12},{14,13},{17,16},{18,1... | collective-permute-start | bytes 1572872 | tf_op jit(solution)/shard_map/ppermute | solution.py:15
  33.6 15.7 %collective-permute-start.2 = (bf16[128,2048]{1,0:T(8,128)(2,1)}, bf16[128,2048]{1,0:T(8,128)(2,1)}, u32[]{:S(2)}, u32[]{:S(2)}) collective-permute-start(bf16[128,2048]{1,0:T(8,128)(2,1)} %collective-permute-done.1), channel_id=1, source_target_pairs={{1,2},{2,3},{5,6},{6,7},{9,10},{10,11},{13,14},{14,15},{17,18},{18... | collective-permute-start | bytes 1572872 | tf_op jit(solution)/shard_map/ppermute | solution.py:15
  48.0 14.9 %collective-permute-start.6 = (bf16[128,2048]{1,0:T(8,128)(2,1)}, bf16[128,2048]{1,0:T(8,128)(2,1)S(1)}, u32[]{:S(2)}, u32[]{:S(2)}) collective-permute-start(bf16[128,2048]{1,0:T(8,128)(2,1)} %collective-permute-done.5), channel_id=1, source_target_pairs={{1,0},{5,4},{9,8},{13,12},{17,16},{21,20},{25,24},{29,28}} | collective-permute-start | bytes 1572872 | tf_op jit(solution)/shard_map/ppermute | solution.py:15
  49.3 13.7 %collective-permute-start.3 = (bf16[128,2048]{1,0:T(8,128)(2,1)}, bf16[128,2048]{1,0:T(8,128)(2,1)S(1)}, u32[]{:S(2)}, u32[]{:S(2)}) collective-permute-start(bf16[128,2048]{1,0:T(8,128)(2,1)} %collective-permute-done.2), channel_id=1, source_target_pairs={{2,3},{6,7},{10,11},{14,15},{18,19},{22,23},{26,27},{30,31}} | collective-permute-start | bytes 1572872 | tf_op jit(solution)/shard_map/ppermute | solution.py:15
  50.0 13.0 %copy-start.9 = (bf16[128,2048]{1,0:T(8,128)(2,1)S(1)}, bf16[128,2048]{1,0:T(8,128)(2,1)}, u32[]{:S(2)}) copy-start(bf16[128,2048]{1,0:T(8,128)(2,1)} %copy-done.8) | copy-start | bytes 1572868
  54.0 9.1 %copy-start.12 = (pred[4,2,32,2,128]{4,3,2,1,0:T(4,128)(4,1)S(1)}, pred[4,2,32,2,128]{4,3,2,1,0:T(4,128)(4,1)}, u32[]{:S(2)}) copy-start(pred[4,2,32,2,128]{4,3,2,1,0:T(4,128)(4,1)} %get-tuple-element.31) | copy-start | bytes 196612
  64.6 18.7 %all-to-all-start.2 = ((bf16[4,64,2048]{2,1,0:T(8,128)(2,1)}), bf16[4,64,2048]{2,1,0:T(8,128)(2,1)}, u32[]{:S(2)}, u32[]{:S(2)}) async-start(bf16[4,64,2048]{2,1,0:T(8,128)(2,1)} %bitcast.209), calls=%async_computation.2 | async-start | bytes 2097152 | tf_op jit(solution)/shard_map/all_to_all | solution.py:163
  68.8 2.0 %copy-start.11 = (pred[4,2,32,2,128]{4,3,2,1,0:T(4,128)(4,1)S(1)}, pred[4,2,32,2,128]{4,3,2,1,0:T(4,128)(4,1)}, u32[]{:S(2)}) copy-start(pred[4,2,32,2,128]{4,3,2,1,0:T(4,128)(4,1)} %get-tuple-element.30) | copy-start | bytes 196612
  73.3 57.9 %collective-permute-start.8 = (bf16[1024,256]{0,1:T(8,128)(2,1)}, bf16[1024,256]{0,1:T(8,128)(2,1)}, u32[]{:S(2)}, u32[]{:S(2)}) collective-permute-start(bf16[1024,256]{0,1:T(8,128)(2,1)} %fusion.48), channel_id=1, source_target_pairs={{0,1},{1,2},{2,3},{4,5},{5,6},{6,7},{8,9},{9,10},{10,11},{12,13},{... | collective-permute-start | bytes 1572872 | tf_op jit(solution)/shard_map/ppermute | solution.py:15
  76.7 56.0 %collective-permute-start.7 = (bf16[1024,256]{0,1:T(8,128)(2,1)}, bf16[1024,256]{0,1:T(8,128)(2,1)}, u32[]{:S(2)}, u32[]{:S(2)}) collective-permute-start(bf16[1024,256]{0,1:T(8,128)(2,1)} %fusion.48), channel_id=1, source_target_pairs={{1,0},{2,1},{3,2},{5,4},{6,5},{7,6},{9,8},{10,9},{11,10},{13,12},{... | collective-permute-start | bytes 1572872 | tf_op jit(solution)/shard_map/ppermute | solution.py:15
  83.3 17.9 %all-to-all-start = ((bf16[4,64,2048]{2,1,0:T(8,128)(2,1)}), bf16[4,64,2048]{2,1,0:T(8,128)(2,1)S(1)}, u32[]{:S(2)}, u32[]{:S(2)}) async-start(bf16[4,64,2048]{2,1,0:T(8,128)(2,1)} %bitcast.13), calls=%async_computation | async-start | bytes 2097152 | tf_op jit(solution)/shard_map/all_to_all | solution.py:163
  101.2 1.0 copy-start.6
  102.2 17.9 %all-to-all-start.3 = ((bf16[4,64,2048]{2,1,0:T(8,128)(2,1)}), bf16[4,64,2048]{2,1,0:T(8,128)(2,1)S(1)}, u32[]{:S(2)}, u32[]{:S(2)}) async-start(bf16[4,64,2048]{2,1,0:T(8,128)(2,1)} %bitcast.212), calls=%async_computation.3 | async-start | bytes 2097152 | tf_op jit(solution)/shard_map/all_to_all | solution.py:167
  120.1 1.0 copy-start.1
  121.1 17.9 %all-to-all-start.1 = ((bf16[4,64,2048]{2,1,0:T(8,128)(2,1)}), bf16[4,64,2048]{2,1,0:T(8,128)(2,1)S(1)}, u32[]{:S(2)}, u32[]{:S(2)}) async-start(bf16[4,64,2048]{2,1,0:T(8,128)(2,1)} %bitcast.208), calls=%async_computation.1 | async-start | bytes 2097152 | tf_op jit(solution)/shard_map/all_to_all | solution.py:167
  124.6 1.7 copy-start.2
  127.8 14.7 %collective-permute-start.13 = (bf16[128,2048]{1,0:T(8,128)(2,1)}, bf16[128,2048]{1,0:T(8,128)(2,1)}, u32[]{:S(2)}, u32[]{:S(2)}) collective-permute-start(bf16[128,2048]{1,0:T(8,128)(2,1)} %get-tuple-element.32), channel_id=1, source_target_pairs={{0,1},{4,5},{8,9},{12,13},{16,17},{20,21},{24,25},{28,29}} | collective-permute-start | bytes 1572872 | tf_op jit(solution)/shard_map/ppermute | solution.py:15
  131.3 30.4 %collective-permute-start.9 = (bf16[1024,256]{0,1:T(8,128)(2,1)}, bf16[1024,256]{0,1:T(8,128)(2,1)}, u32[]{:S(2)}, u32[]{:S(2)}) collective-permute-start(bf16[1024,256]{0,1:T(8,128)(2,1)} %collective-permute-done.8), channel_id=1, source_target_pairs={{1,2},{2,3},{5,6},{6,7},{9,10},{10,11},{13,14},{14,15},{17,18},{18... | collective-permute-start | bytes 1572872 | tf_op jit(solution)/shard_map/ppermute | solution.py:15
  132.7 29.7 %collective-permute-start.11 = (bf16[1024,256]{0,1:T(8,128)(2,1)}, bf16[1024,256]{0,1:T(8,128)(2,1)}, u32[]{:S(2)}, u32[]{:S(2)}) collective-permute-start(bf16[1024,256]{0,1:T(8,128)(2,1)} %collective-permute-done.7), channel_id=1, source_target_pairs={{1,0},{2,1},{5,4},{6,5},{9,8},{10,9},{13,12},{14,13},{17,16},{18,1... | collective-permute-start | bytes 1572872 | tf_op jit(solution)/shard_map/ppermute | solution.py:15
  142.5 6.1 %copy-start.3 = (bf16[4,64,2048]{2,1,0:T(8,128)(2,1)S(1)}, bf16[4,64,2048]{2,1,0:T(8,128)(2,1)}, u32[]{:S(2)}) copy-start(bf16[4,64,2048]{2,1,0:T(8,128)(2,1)} %copy-done.1) | copy-start | bytes 3145732
  142.5 6.1 %copy-start.10 = (bf16[128,256]{0,1:T(8,128)(2,1)S(1)}, bf16[128,256]{0,1:T(8,128)(2,1)}, u32[]{:S(2)}) copy-start(bf16[128,256]{0,1:T(8,128)(2,1)} %get-tuple-element.18) | copy-start | bytes 196612
  144.0 15.3 %collective-permute-start.14 = (bf16[128,2048]{1,0:T(8,128)(2,1)S(1)}, bf16[128,2048]{1,0:T(8,128)(2,1)S(1)}, u32[]{:S(2)}, u32[]{:S(2)}) collective-permute-start(bf16[128,2048]{1,0:T(8,128)(2,1)S(1)} %get-tuple-element.34), channel_id=1, source_target_pairs={{0,1},{1,2},{4,5},{5,6},{8,9},{9,10},{12,13},{13,14},{16,17},{17,1... | collective-permute-start | bytes 1572872 | tf_op jit(solution)/shard_map/ppermute | solution.py:15
  149.3 10.8 %copy-start.5 = (bf16[1024,512]{1,0:T(8,128)(2,1)S(1)}, bf16[1024,512]{1,0:T(8,128)(2,1)}, u32[]{:S(2)}) copy-start(bf16[1024,512]{1,0:T(8,128)(2,1)} %param.14) | copy-start | bytes 3145732
  159.5 4.6 %collective-permute-start.16 = (bf16[128,2048]{1,0:T(8,128)(2,1)S(1)}, bf16[128,2048]{1,0:T(8,128)(2,1)S(1)}, u32[]{:S(2)}, u32[]{:S(2)}) collective-permute-start(bf16[128,2048]{1,0:T(8,128)(2,1)S(1)} %get-tuple-element.7), channel_id=1, source_target_pairs={{3,2},{7,6},{11,10},{15,14},{19,18},{23,22},{27,26},{31,30}} | collective-permute-start | bytes 1572872 | tf_op jit(solution)/shard_map/ppermute | solution.py:15
  161.7 11.8 %collective-permute-start.10 = (bf16[1024,256]{0,1:T(8,128)(2,1)}, bf16[1024,256]{0,1:T(8,128)(2,1)S(1)}, u32[]{:S(2)}, u32[]{:S(2)}) collective-permute-start(bf16[1024,256]{0,1:T(8,128)(2,1)} %collective-permute-done.9), channel_id=1, source_target_pairs={{2,3},{6,7},{10,11},{14,15},{18,19},{22,23},{26,27},{30,31}} | collective-permute-start | bytes 1572872 | tf_op jit(solution)/shard_map/ppermute | solution.py:15
  162.4 14.8 %collective-permute-start.12 = (bf16[1024,256]{0,1:T(8,128)(2,1)}, bf16[1024,256]{0,1:T(8,128)(2,1)S(1)}, u32[]{:S(2)}, u32[]{:S(2)}) collective-permute-start(bf16[1024,256]{0,1:T(8,128)(2,1)} %collective-permute-done.11), channel_id=1, source_target_pairs={{1,0},{5,4},{9,8},{13,12},{17,16},{21,20},{25,24},{29,28}} | collective-permute-start | bytes 1572872 | tf_op jit(solution)/shard_map/ppermute | solution.py:15
  164.2 7.9 %collective-permute-start.17 = (bf16[128,2048]{1,0:T(8,128)(2,1)S(1)}, bf16[128,2048]{1,0:T(8,128)(2,1)S(1)}, u32[]{:S(2)}, u32[]{:S(2)}) collective-permute-start(bf16[128,2048]{1,0:T(8,128)(2,1)S(1)} %add_convert_fusion.3), channel_id=1, source_target_pairs={{2,1},{3,2},{6,5},{7,6},{10,9},{11,10},{14,13},{15,14},{18,17},{19... | collective-permute-start | bytes 1572872 | tf_op jit(solution)/shard_map/ppermute | solution.py:15
  165.2 6.9 %copy-start.4 = (f32[128,2048]{1,0:T(8,128)S(1)}, f32[128,2048]{1,0:T(8,128)}, u32[]{:S(2)}) copy-start(f32[128,2048]{1,0:T(8,128)} %get-tuple-element.33) | copy-start | bytes 3145732
  166.9 15.1 %collective-permute-start.15 = (bf16[128,2048]{1,0:T(8,128)(2,1)S(1)}, bf16[128,2048]{1,0:T(8,128)(2,1)S(1)}, u32[]{:S(2)}, u32[]{:S(2)}) collective-permute-start(bf16[128,2048]{1,0:T(8,128)(2,1)S(1)} %get-tuple-element.6), channel_id=1, source_target_pairs={{0,1},{1,2},{2,3},{4,5},{5,6},{6,7},{8,9},{9,10},{10,11},{12,13},{... | collective-permute-start | bytes 1572872 | tf_op jit(solution)/shard_map/ppermute | solution.py:15
  172.2 28.7 %collective-permute-start.18 = (bf16[128,2048]{1,0:T(8,128)(2,1)S(1)}, bf16[128,2048]{1,0:T(8,128)(2,1)S(1)}, u32[]{:S(2)}, u32[]{:S(2)}) collective-permute-start(bf16[128,2048]{1,0:T(8,128)(2,1)S(1)} %add_convert_fusion.2), channel_id=1, source_target_pairs={{1,0},{2,1},{3,2},{5,4},{6,5},{7,6},{9,8},{10,9},{11,10},{13,12},{... | collective-permute-start | bytes 1572872 | tf_op jit(solution)/shard_map/ppermute | solution.py:15

commit v2 on v1

v2 whole, which is shorter than its diff:
```python
import jax
import jax.numpy as jnp
from jax import lax
from jax.sharding import PartitionSpec as P

epsilon = 1e-06
halo_depth = 16
f32 = jnp.float32
bf16 = jnp.bfloat16


def moved(block, axis, by, keep):
    size = lax.axis_size(axis)
    pairs = [(i, i + by) for i in range(size) if 0 <= i + by < size and keep(i)]
    return lax.ppermute(block, axis, pairs)


def offset_blocks(block, from_left, from_right, axis):
    size = lax.axis_size(axis)
    own = lax.axis_index(axis)
    blocks = [block]
    for m in range(1, size):
        blocks.append(jnp.where(own + m < size, from_right[m], from_left[size - m]))
    return blocks


def gather_step(step, from_left, from_right, axis):
    size = lax.axis_size(axis)
    to_right, to_left = lax.optimization_barrier((from_left[-1], from_right[-1]))
    from_left.append(moved(to_right, axis, 1, lambda i: i >= step - 1))
    from_right.append(moved(to_left, axis, -1, lambda i: i <= size - step))


def after(value, *others):
    return lax.optimization_barrier((value,) + others)[0]


def expert_rows(received, gate_weight, up_weight, down_weight):
    shape_in = received.shape
    flat_rows = received.reshape(-1, shape_in[-1])
    gate_part = jnp.dot(flat_rows, gate_weight[0], preferred_element_type=f32)
    up_part = jnp.dot(flat_rows, up_weight[0], preferred_element_type=f32)
    hidden = (jax.nn.silu(gate_part) * up_part).astype(bf16)
    result = jnp.dot(hidden, down_weight[0], preferred_element_type=f32).astype(bf16)
    return result.reshape(shape_in)


def pool_mapped(pool_input, pool_map, pool_scale):
    row_count, width_local = pool_input.shape
    group_dim = pool_map.shape[1]
    groups_local = width_local // group_dim
    last_rows = pool_input[row_count - halo_depth :]
    earlier_rows = moved(last_rows, "ep", 1, lambda i: True)
    extended = jnp.concatenate([earlier_rows, pool_input], axis=0).astype(f32)
    first_group = lax.axis_index("tp") * groups_local
    group_ids = first_group + jnp.arange(width_local, dtype=jnp.int32) // group_dim
    window = jnp.left_shift(jnp.int32(2), group_ids % 4)
    summed = jnp.zeros((row_count, width_local), f32)
    for offset in range(halo_depth):
        shifted = extended[halo_depth - offset : halo_depth - offset + row_count]
        summed = summed + jnp.where(offset < window, shifted, 0.0)
    positions = lax.axis_index("ep") * row_count + jnp.arange(row_count, dtype=jnp.int32)
    counted = jnp.minimum(positions[:, None] + 1, window[None, :]).astype(f32)
    pooled = (summed / counted - extended[halo_depth:]).astype(bf16)
    maps_local = lax.dynamic_slice_in_dim(pool_map, first_group, groups_local, 0)
    scales_local = lax.dynamic_slice_in_dim(pool_scale, first_group * group_dim, width_local, 0)
    mapped = jnp.einsum(
        "rgc,gcd->rgd",
        pooled.reshape(row_count, groups_local, group_dim),
        maps_local,
        preferred_element_type=f32,
    )
    return (mapped.reshape(row_count, width_local) * scales_local).astype(bf16)


def pool_project(blocks, out_weight):
    size = len(blocks)
    depth = blocks[0].shape[1]
    own = lax.axis_index("tp")
    total = None
    for m in range(size):
        rows = lax.dynamic_slice_in_dim(out_weight, (own + m) % size * depth, depth, 0)
        product = jnp.dot(blocks[m], rows, preferred_element_type=f32)
        total = product if total is None else total + product
    return total.astype(bf16)


def on_device(
    pool_input,
    pool_map,
    pool_scale,
    out_weight,
    expert_input,
    norm_gain,
    routes,
    route_weight,
    gate_weight,
    up_weight,
    down_weight,
):
    row_count, model_width = expert_input.shape
    top_count = routes.shape[1]
    ep_count = lax.axis_size("ep")
    tp_count = lax.axis_size("tp")
    capacity = 2 * row_count * top_count // (ep_count * tp_count)
    experts = ep_count * tp_count
    parts = 2 if capacity % 2 == 0 else 1
    depth = capacity // parts

    widened = expert_input.astype(f32)
    normed = (
        widened
        * lax.rsqrt(jnp.mean(widened * widened, axis=1, keepdims=True) + epsilon)
        * norm_gain
    ).astype(bf16)

    named = jnp.arange(experts, dtype=jnp.int32)
    match = routes.T[:, None, :] == named[None, :, None]
    chosen = match.any(axis=0)
    scale = jnp.where(match, route_weight.T[:, None, :], 0.0).sum(axis=0)
    count = jnp.arange(row_count, dtype=jnp.int32)
    earlier = (count[:, None] < count[None, :]).astype(bf16)
    rank = jnp.dot(chosen.astype(bf16), earlier, preferred_element_type=f32).astype(jnp.int32)
    rank = jnp.where(chosen, rank, capacity)

    def taken(part):
        slots = part * depth + jnp.arange(depth, dtype=jnp.int32)
        return rank[:, None, :] == slots[None, :, None]

    def exchanged(rows):
        shape = rows.shape
        rows = rows.reshape(experts, depth, model_width)
        rows = lax.all_to_all(rows, ("ep", "tp"), split_axis=0, concat_axis=0, tiled=True)
        return rows.reshape(shape)

    received = []
    for part in range(parts):
        select = taken(part).astype(bf16).reshape(experts * depth, row_count)
        outgoing = jnp.dot(select, normed, preferred_element_type=f32).astype(bf16)
        received.append(exchanged(outgoing))

    mapped = pool_mapped(pool_input, pool_map, pool_scale)
    pool_left, pool_right = [mapped], [mapped]
    for step in range(1, tp_count):
        gather_step(step, pool_left, pool_right, "tp")

    total = None
    for part in range(parts):
        results = expert_rows(received[part], gate_weight, up_weight, down_weight)
        returned = exchanged(results)
        weighted = jnp.where(taken(part), scale[:, None, :], 0.0)
        weighted = weighted.reshape(experts * depth, row_count).T
        upper = weighted.astype(bf16)
        lower = (weighted - upper.astype(f32)).astype(bf16)
        product = jnp.dot(upper, returned, preferred_element_type=f32)
        product = product + jnp.dot(lower, returned, preferred_element_type=f32)
        total = product if total is None else total + product

    pool_blocks = offset_blocks(mapped, pool_left, pool_right, "tp")
    return (pool_project(pool_blocks, out_weight), total.astype(bf16))


def solution(mesh):
    return jax.shard_map(
        on_device,
        mesh=mesh,
        in_specs=(
            P(("grp", "ep"), "tp"),
            P(),
            P(),
            P(None, "tp"),
            P(("grp", "ep", "tp"), None),
            P(),
            P(("grp", "ep", "tp"), None),
            P(("grp", "ep", "tp"), None),
            P(("ep", "tp"), None, None),
            P(("ep", "tp"), None, None),
            P(("ep", "tp"), None, None),
        ),
        out_specs=(P(("grp", "ep"), "tp"), P(("grp", "ep", "tp"), None)),
        check_vma=False,
    )
```

time: 203 us -> 169 us (0.83)
  blocking collectives: 12 us -> 0 us
  starting transfers between devices: 53.9 us -> 42.7 us
  other arithmetic: 14.2 us -> 4.96 us
  waiting for transfers between devices: 80 us -> 75 us
  matrix products: 36.8 us -> 41.4 us
    ppermute x19 -> x7, starting transfers between devices: 39.1 us -> 13.6 us  [moved(): return lax.ppermute(block, axis, pairs)]
    ppermute x19 -> x7, waiting for transfers between devices: 56.4 us -> 36.5 us  [moved(): return lax.ppermute(block, axis, pairs)]
    all_to_all x4, waiting for transfers between devices: 23.6 us -> 38.4 us  [exchanged(): lax.all_to_all(rows, ('ep', 'tp'), split_axis=0, concat_axis=0, tiled=True)]
    all_to_all x4, starting transfers between devices: 14.8 us -> 29.1 us  [exchanged(): lax.all_to_all(rows, ('ep', 'tp'), split_axis=0, concat_axis=0, tiled=True)]
    all_gather x1 -> x0, blocking collectives: 12 us -> none  [on_device(): facts = lax.all_gather(facts, 'tp', axis=0, tiled=False)]
    dot_general x1, matrix products: 3.94 us -> 11.9 us  [pool_mapped(): jnp.einsum('rgc,gcd->rgd', pooled.reshape(row_count, groups_local, group_...]
    convert_element_type x7 -> x0, other arithmetic: 4.06 us -> none  [the longest x1 2.04 us: on_device(): normed = (widened * lax.rsqrt(jnp.mean(widened * widened, axis=1, keepdim...]
    gt x8, other arithmetic: 3.52 us -> 0.13 us  [pool_mapped(): summed = summed + jnp.where(offset < window, shifted, 0.0)]
  transfers between devices with their start and end apart: 23 -> 11, of which waited for: 11 -> 5; matrix products, arithmetic and copies ran while one was open for 23% -> 23% of each run, Pallas kernels for 0% -> 0%
where the time goes in v2:
time: 169 us; the launch traced here: 168 us
  waiting for transfers between devices  75 us (44%)
  starting transfers between devices  42.7 us (25%)
  matrix products  41.4 us (24%)
  other arithmetic  4.96 us (3%)
  local copies, waits for them, and re-layouts  2.68 us (2%)
    all_to_all x4, waiting for transfers between devices, exchanged(): lax.all_to_all(rows, ('ep', 'tp'), split_axis=0, concat_axis=0, tiled=True)  38.4 us
    ppermute x7, waiting for transfers between devices, moved(): return lax.ppermute(block, axis, pairs)  36.5 us
    all_to_all x4, starting transfers between devices, exchanged(): lax.all_to_all(rows, ('ep', 'tp'), split_axis=0, concat_axis=0, tiled=True)  29.1 us
    ppermute x7, starting transfers between devices, moved(): return lax.ppermute(block, axis, pairs)  13.6 us
    dot_general x1, matrix products, pool_mapped(): jnp.einsum('rgc,gcd->rgd', pooled.reshape(row_count, groups_local, group_...  11.9 us
    dot_general x2, matrix products, expert_rows(): jnp.dot(hidden, down_weight[0], preferred_element_type=f32).astype(bf16)  8.6 us
    dot_general x4, matrix products, pool_project(): product = jnp.dot(blocks[m], rows, preferred_element_type=f32)  6.13 us
    dot_general x2, matrix products, expert_rows(): gate_part = jnp.dot(flat_rows, gate_weight[0], preferred_element_type=f32)  4.94 us
  transfers between devices with their start and end apart: 11, of which 5 were waited for; matrix products, arithmetic and copies ran while one was open for 23% of the time, Pallas kernels for 0%

profile of v2, /device:TPU:0, one launch (start us, length us, event | category | flops | bytes accessed | tf_op | source)
XLA Modules:
  0.0 167.8 jit_solution(13538593911165345219)
XLA Ops:
  0.6 0.0 copy-start
  0.7 0.8 fusion.88
  1.5 0.1 fusion.24
  1.6 0.1 eq.82
  1.7 0.1 eq.78
  1.8 1.3 fusion.25
  3.1 0.1 bitcast_compare_fusion
  3.3 2.5 %convolution_convert_fusion.3 = bf16[256,2048]{1,0:T(8,128)(2,1)} fusion(pred[256,128]{1,0:T(32,128)(4,1)S(1)} %get-tuple-element.19, bf16[128,2048]{1,0:T(8,128)(2,1)} %param.15, f32[2048]{0:T(1024)} %param.16, f32[128]{0:T(128)S(1)} %add_rsqrt_fusion), kind=kOutput, calls=%fused_computation.3 | convolution fusion | flops 135790592 | bytes 1614336 | tf_op jit(solution)/shard_map/dot_general | solution.py:139
  5.8 7.5 %all-to-all-start = ((bf16[16,16,2048]{2,1,0:T(8,128)(2,1)}), bf16[16,16,2048]{2,1,0:T(8,128)(2,1)}, u32[]{:S(2)}, u32[]{:S(2)}) async-start(bf16[16,16,2048]{2,1,0:T(8,128)(2,1)} %bitcast.117), calls=%async_computation | async-start | bytes 2097152 | tf_op jit(solution)/shard_map/all_to_all | solution.py:133
  13.3 0.7 slice.52
  14.0 2.2 %collective-permute-start = (bf16[16,256]{1,0:T(8,128)(2,1)S(1)}, bf16[16,256]{1,0:T(8,128)(2,1)S(1)}, u32[]{:S(2)}, u32[]{:S(2)}) collective-permute-start(bf16[16,256]{1,0:T(8,128)(2,1)S(1)} %slice.52), channel_id=1, source_target_pairs={{0,4},{4,8},{8,12},{1,5},{5,9},{9,13},{2,6},{6,10},{10,14},{3,7},{... | collective-permute-start | bytes 24584 | tf_op jit(solution)/shard_map/ppermute | solution.py:15
  16.3 1.5 convolution_convert_fusion.1
  17.8 22.4 %all-to-all-done = bf16[16,16,2048]{2,1,0:T(8,128)(2,1)} async-done(((bf16[16,16,2048]{2,1,0:T(8,128)(2,1)}), bf16[16,16,2048]{2,1,0:T(8,128)(2,1)}, u32[]{:S(2)}, u32[]{:S(2)}) %all-to-all-start) | async-done | bytes 1048608 | tf_op jit(solution)/shard_map/all_to_all | solution.py:133
  40.2 3.7 %all-to-all-start.2 = ((bf16[16,16,2048]{2,1,0:T(8,128)(2,1)}), bf16[16,16,2048]{2,1,0:T(8,128)(2,1)S(1)}, u32[]{:S(2)}, u32[]{:S(2)}) async-start(bf16[16,16,2048]{2,1,0:T(8,128)(2,1)} %bitcast.116), calls=%async_computation.2 | async-start | bytes 2097152 | tf_op jit(solution)/shard_map/all_to_all | solution.py:133
  44.0 0.8 dynamic_slice.19
  44.7 2.1 %maximum_convert_fusion = f32[1040,256]{1,0:T(8,128)} fusion(bf16[1024,256]{1,0:T(8,128)(2,1)} %param.11, bf16[16,256]{1,0:T(8,128)(2,1)S(1)} %collective-permute-done), kind=kLoop, calls=%fused_computation.65 | loop fusion | flops 1064960 | bytes 1597440 | tf_op jit(solution)/shard_map/convert_element_type | solution.py:54
  46.9 3.4 %fusion.10 = f32[256,512]{1,0:T(8,128)} fusion(bf16[256,2048]{1,0:T(8,128)(2,1)} %bitcast.8, bf16[1,2048,512]{2,1,0:T(8,128)(2,1)} %param.19), kind=kOutput, calls=%fused_computation.16 | convolution fusion | flops 536870912 | bytes 3670016 | tf_op jit(solution)/shard_map/dot_general | solution.py:41
  50.3 4.3 %convolution_convert_fusion.2 = bf16[256,2048]{1,0:T(8,128)(2,1)} fusion(bf16[1,512,2048]{2,1,0:T(8,128)(2,1)S(1)} %copy-done, bf16[256,2048]{1,0:T(8,128)(2,1)} %bitcast.8, bf16[1,2048,512]{2,1,0:T(8,128)(2,1)} %param.20, f32[256,512]{1,0:T(8,128)} %fusion.10), kind=kOutput, calls=%fused_computation.2 | convolution fusion | flops 1075052544 | bytes 6815744 | tf_op jit(solution)/shard_map/dot_general | solution.py:44
  54.6 16.1 %all-to-all-done.2 = bf16[16,16,2048]{2,1,0:T(8,128)(2,1)S(1)} async-done(((bf16[16,16,2048]{2,1,0:T(8,128)(2,1)}), bf16[16,16,2048]{2,1,0:T(8,128)(2,1)S(1)}, u32[]{:S(2)}, u32[]{:S(2)}) %all-to-all-start.2) | async-done | bytes 1048608 | tf_op jit(solution)/shard_map/all_to_all | solution.py:133
  70.7 1.0 copy-done.5
  71.6 3.7 %all-to-all-start.1 = ((bf16[16,16,2048]{2,1,0:T(8,128)(2,1)}), bf16[16,16,2048]{2,1,0:T(8,128)(2,1)S(1)}, u32[]{:S(2)}, u32[]{:S(2)}) async-start(bf16[16,16,2048]{2,1,0:T(8,128)(2,1)} %bitcast.121), calls=%async_computation.1 | async-start | bytes 2097152 | tf_op jit(solution)/shard_map/all_to_all | solution.py:133
  75.3 0.0 copy-start.10
  75.3 11.9 %fusion.51 = f32[2,128,1024]{2,1,0:T(8,128)S(1)} fusion(bf16[8,128,128]{2,1,0:T(8,128)(2,1)} %param.12, s32[]{:T(128)S(6)} %select_n.142, s32[256]{0:T(256)S(1)} %fusion.94, s32[1024]{0:T(1024)S(1)} %add_add_fusion, f32[1040,256]{1,0:T(8,128)} %maximum_convert_fusion, pred[256]{0:T(512)(128)(4,1)S(1)} %get-tuple-element.20, ...), kind=kOutput, calls=%fused_computation.66 | convolution fusion | flops 76546048 | bytes 17900548 | tf_op jit(solution)/shard_map/rgc,gcd->rgd/dot_general | solution.py:67
  87.2 0.1 fusion.45
  87.3 0.0 copy-start.3
  87.3 1.3 collective-permute-start.1
  88.6 5.4 %collective-permute-start.2 = (bf16[1024,256]{0,1:T(8,128)(2,1)S(1)}, bf16[1024,256]{0,1:T(8,128)(2,1)}, u32[]{:S(2)}, u32[]{:S(2)}) collective-permute-start(bf16[1024,256]{0,1:T(8,128)(2,1)S(1)} %fusion.45), channel_id=1, source_target_pairs={{0,1},{1,2},{2,3},{4,5},{5,6},{6,7},{8,9},{9,10},{10,11},{12,13},{... | collective-permute-start | bytes 1572872 | tf_op jit(solution)/shard_map/ppermute | solution.py:15
  94.0 12.5 %collective-permute-done.1 = bf16[1024,256]{0,1:T(8,128)(2,1)} collective-permute-done((bf16[1024,256]{0,1:T(8,128)(2,1)S(1)}, bf16[1024,256]{0,1:T(8,128)(2,1)}, u32[]{:S(2)}, u32[]{:S(2)}) %collective-permute-start.1) | collective-permute-done | bytes 524320 | tf_op jit(solution)/shard_map/ppermute | solution.py:15
  106.5 1.4 collective-permute-start.3
  107.9 1.3 collective-permute-start.4
  109.3 1.5 fusion.8
  110.8 4.3 %convolution_convert_fusion = bf16[256,2048]{1,0:T(8,128)(2,1)} fusion(bf16[1,512,2048]{2,1,0:T(8,128)(2,1)S(1)} %copy-done, bf16[256,2048]{1,0:T(8,128)(2,1)} %bitcast.119, bf16[1,2048,512]{2,1,0:T(8,128)(2,1)} %param.20, f32[256,512]{1,0:T(8,128)} %fusion.8), kind=kOutput, calls=%fused_computation | convolution fusion | flops 1075052544 | bytes 6815744 | tf_op jit(solution)/shard_map/dot_general | solution.py:44
  115.1 14.4 %all-to-all-start.3 = ((bf16[16,16,2048]{2,1,0:T(8,128)(2,1)}), bf16[16,16,2048]{2,1,0:T(8,128)(2,1)}, u32[]{:S(2)}, u32[]{:S(2)}) async-start(bf16[16,16,2048]{2,1,0:T(8,128)(2,1)} %bitcast.118), calls=%async_computation.3 | async-start | bytes 2097152 | tf_op jit(solution)/shard_map/all_to_all | solution.py:133
  129.5 0.1 bitcast_convert_fusion
  129.7 0.1 fusion.85
  129.9 0.0 copy-start.4
  129.9 0.9 collective-permute-done.4
  130.8 0.7 collective-permute-start.5
  131.5 1.6 fusion.81
  133.1 1.3 collective-permute-start.6
  134.4 1.5 fusion.68
  136.0 1.5 fusion.70
  137.5 23.1 %collective-permute-done.6 = bf16[1024,256]{0,1:T(8,128)(2,1)S(1)} collective-permute-done((bf16[1024,256]{0,1:T(8,128)(2,1)}, bf16[1024,256]{0,1:T(8,128)(2,1)S(1)}, u32[]{:S(2)}, u32[]{:S(2)}) %collective-permute-start.6) | collective-permute-done | bytes 524320 | tf_op jit(solution)/shard_map/ppermute | solution.py:15
  160.6 1.5 add_convert_fusion
  162.1 0.3 fusion.99
  162.4 1.3 convolution_add_fusion.1
  163.7 1.6 fusion.100
  165.4 2.4 %fusion.1 = bf16[128,2048]{1,0:T(8,128)(2,1)} fusion(f32[128,2048]{1,0:T(8,128)S(1)} %copy-done.2, f32[128,2048]{1,0:T(8,128)S(1)} %fusion.100, bf16[128,256]{0,1:T(8,128)(2,1)S(1)} %get-tuple-element.14, bf16[256,2048]{1,0:T(8,128)(2,1)} %bitcast.18), kind=kOutput, calls=%fused_computation.7 | convolution fusion | flops 135004160 | bytes 3735552 | tf_op jit(solution)/shard_map/dot_general | solution.py:156
  (38 shorter events, 0.2 us)
Async XLA Ops:
  0.6 49.7 %copy-start = (bf16[1,512,2048]{2,1,0:T(8,128)(2,1)S(1)}, bf16[1,512,2048]{2,1,0:T(8,128)(2,1)}, u32[]{:S(2)}) copy-start(bf16[1,512,2048]{2,1,0:T(8,128)(2,1)} %param.21) | copy-start | bytes 6291460
  1.8 14.5 %copy-start.1 = (bf16[128,2048]{1,0:T(8,128)(2,1)S(1)}, bf16[128,2048]{1,0:T(8,128)(2,1)}, u32[]{:S(2)}) copy-start(bf16[128,2048]{1,0:T(8,128)(2,1)} %param.15) | copy-start | bytes 1572868
  1.8 14.5 %copy-start.7 = (f32[2048]{0:T(1024)S(1)}, f32[2048]{0:T(1024)}, u32[]{:S(2)}) copy-start(f32[2048]{0:T(1024)} %param.16) | copy-start | bytes 24580
  5.8 34.4 %all-to-all-start = ((bf16[16,16,2048]{2,1,0:T(8,128)(2,1)}), bf16[16,16,2048]{2,1,0:T(8,128)(2,1)}, u32[]{:S(2)}, u32[]{:S(2)}) async-start(bf16[16,16,2048]{2,1,0:T(8,128)(2,1)} %bitcast.117), calls=%async_computation | async-start | bytes 2097152 | tf_op jit(solution)/shard_map/all_to_all | solution.py:133
  14.0 30.8 %collective-permute-start = (bf16[16,256]{1,0:T(8,128)(2,1)S(1)}, bf16[16,256]{1,0:T(8,128)(2,1)S(1)}, u32[]{:S(2)}, u32[]{:S(2)}) collective-permute-start(bf16[16,256]{1,0:T(8,128)(2,1)S(1)} %slice.52), channel_id=1, source_target_pairs={{0,4},{4,8},{8,12},{1,5},{5,9},{9,13},{2,6},{6,10},{10,14},{3,7},{... | collective-permute-start | bytes 24584 | tf_op jit(solution)/shard_map/ppermute | solution.py:15
  40.2 30.5 %all-to-all-start.2 = ((bf16[16,16,2048]{2,1,0:T(8,128)(2,1)}), bf16[16,16,2048]{2,1,0:T(8,128)(2,1)S(1)}, u32[]{:S(2)}, u32[]{:S(2)}) async-start(bf16[16,16,2048]{2,1,0:T(8,128)(2,1)} %bitcast.116), calls=%async_computation.2 | async-start | bytes 2097152 | tf_op jit(solution)/shard_map/all_to_all | solution.py:133
  70.6 1.0 copy-start.5
  71.6 43.4 %all-to-all-start.1 = ((bf16[16,16,2048]{2,1,0:T(8,128)(2,1)}), bf16[16,16,2048]{2,1,0:T(8,128)(2,1)S(1)}, u32[]{:S(2)}, u32[]{:S(2)}) async-start(bf16[16,16,2048]{2,1,0:T(8,128)(2,1)} %bitcast.121), calls=%async_computation.1 | async-start | bytes 2097152 | tf_op jit(solution)/shard_map/all_to_all | solution.py:133
  75.3 33.9 %copy-start.6 = (bf16[16,16,2048]{2,1,0:T(8,128)(2,1)S(1)}, bf16[16,16,2048]{2,1,0:T(8,128)(2,1)}, u32[]{:S(2)}) copy-start(bf16[16,16,2048]{2,1,0:T(8,128)(2,1)} %copy-done.5) | copy-start | bytes 3145732
  75.3 33.9 %copy-start.10 = (bf16[1,2048,512]{2,1,0:T(8,128)(2,1)S(1)}, bf16[1,2048,512]{2,1,0:T(8,128)(2,1)}, u32[]{:S(2)}) copy-start(bf16[1,2048,512]{2,1,0:T(8,128)(2,1)} %param.19) | copy-start | bytes 6291460
  87.3 1.3 copy-start.3
  87.3 19.2 %collective-permute-start.1 = (bf16[1024,256]{0,1:T(8,128)(2,1)S(1)}, bf16[1024,256]{0,1:T(8,128)(2,1)}, u32[]{:S(2)}, u32[]{:S(2)}) collective-permute-start(bf16[1024,256]{0,1:T(8,128)(2,1)S(1)} %fusion.45), channel_id=1, source_target_pairs={{1,0},{2,1},{3,2},{5,4},{6,5},{7,6},{9,8},{10,9},{11,10},{13,12},{... | collective-permute-start | bytes 1572872 | tf_op jit(solution)/shard_map/ppermute | solution.py:15
  88.6 17.9 %collective-permute-start.2 = (bf16[1024,256]{0,1:T(8,128)(2,1)S(1)}, bf16[1024,256]{0,1:T(8,128)(2,1)}, u32[]{:S(2)}, u32[]{:S(2)}) collective-permute-start(bf16[1024,256]{0,1:T(8,128)(2,1)S(1)} %fusion.45), channel_id=1, source_target_pairs={{0,1},{1,2},{2,3},{4,5},{5,6},{6,7},{8,9},{9,10},{10,11},{12,13},{... | collective-permute-start | bytes 1572872 | tf_op jit(solution)/shard_map/ppermute | solution.py:15
  106.5 23.4 %collective-permute-start.3 = (bf16[1024,256]{0,1:T(8,128)(2,1)}, bf16[1024,256]{0,1:T(8,128)(2,1)}, u32[]{:S(2)}, u32[]{:S(2)}) collective-permute-start(bf16[1024,256]{0,1:T(8,128)(2,1)} %collective-permute-done.2), channel_id=1, source_target_pairs={{1,2},{2,3},{5,6},{6,7},{9,10},{10,11},{13,14},{14,15},{17,18},{18... | collective-permute-start | bytes 1572872 | tf_op jit(solution)/shard_map/ppermute | solution.py:15
  107.9 22.9 %collective-permute-start.4 = (bf16[1024,256]{0,1:T(8,128)(2,1)}, bf16[1024,256]{0,1:T(8,128)(2,1)}, u32[]{:S(2)}, u32[]{:S(2)}) collective-permute-start(bf16[1024,256]{0,1:T(8,128)(2,1)} %collective-permute-done.1), channel_id=1, source_target_pairs={{1,0},{2,1},{5,4},{6,5},{9,8},{10,9},{13,12},{14,13},{17,16},{18,1... | collective-permute-start | bytes 1572872 | tf_op jit(solution)/shard_map/ppermute | solution.py:15
  115.1 14.4 %copy-start.8 = (s32[128,2]{0,1:T(2,128)S(1)}, s32[128,2]{0,1:T(2,128)}, u32[]{:S(2)}) copy-start(s32[128,2]{0,1:T(2,128)} %param.17) | copy-start | bytes 3076
  115.1 14.4 %copy-start.9 = (f32[128,2]{0,1:T(2,128)S(1)}, f32[128,2]{0,1:T(2,128)}, u32[]{:S(2)}) copy-start(f32[128,2]{0,1:T(2,128)} %param.18) | copy-start | bytes 3076
  115.1 48.7 %all-to-all-start.3 = ((bf16[16,16,2048]{2,1,0:T(8,128)(2,1)}), bf16[16,16,2048]{2,1,0:T(8,128)(2,1)}, u32[]{:S(2)}, u32[]{:S(2)}) async-start(bf16[16,16,2048]{2,1,0:T(8,128)(2,1)} %bitcast.118), calls=%async_computation.3 | async-start | bytes 2097152 | tf_op jit(solution)/shard_map/all_to_all | solution.py:133
  129.9 4.5 %copy-start.4 = (bf16[1024,512]{1,0:T(8,128)(2,1)S(1)}, bf16[1024,512]{1,0:T(8,128)(2,1)}, u32[]{:S(2)}) copy-start(bf16[1024,512]{1,0:T(8,128)(2,1)} %param.14) | copy-start | bytes 3145732
  130.8 5.1 %collective-permute-start.5 = (bf16[1024,256]{0,1:T(8,128)(2,1)}, bf16[1024,256]{0,1:T(8,128)(2,1)S(1)}, u32[]{:S(2)}, u32[]{:S(2)}) collective-permute-start(bf16[1024,256]{0,1:T(8,128)(2,1)} %collective-permute-done.3), channel_id=1, source_target_pairs={{2,3},{6,7},{10,11},{14,15},{18,19},{22,23},{26,27},{30,31}} | collective-permute-start | bytes 1572872 | tf_op jit(solution)/shard_map/ppermute | solution.py:15
  133.1 27.5 %collective-permute-start.6 = (bf16[1024,256]{0,1:T(8,128)(2,1)}, bf16[1024,256]{0,1:T(8,128)(2,1)S(1)}, u32[]{:S(2)}, u32[]{:S(2)}) collective-permute-start(bf16[1024,256]{0,1:T(8,128)(2,1)} %collective-permute-done.4), channel_id=1, source_target_pairs={{1,0},{5,4},{9,8},{13,12},{17,16},{21,20},{25,24},{29,28}} | collective-permute-start | bytes 1572872 | tf_op jit(solution)/shard_map/ppermute | solution.py:15
  163.7 1.7 copy-start.2
